TPU v7x, 256 devices: a whole 4x4x8 slice. The times are simulated.
256 devices in a mesh: sp: 16 (over y, x), tp: 16 (over z, core).
Axes of the slice: x: 4, y: 4, z: 8, core: 2. Of those that a mesh axis runs over, the one named last changes fastest.
Arguments:
- upstream: bfloat16 [4096, 4096], P('sp', 'tp'), may hold values from -6 to 6
- stream: bfloat16 [4096, 4096], P('sp', 'tp'), may hold values from -400 to 400
- norm_gain: float32 [4096], P('tp'), may hold values from 0.1 to 1.9
- routes: int32 [4096, 2], P('sp'), may hold values from 0 to 15, all different within a row; in each aligned block of 256 rows (0 to 255, 256 to 511, ...) at most 48 rows name the same one
- route_weights: float32 [4096, 2], P('sp'), may hold values from 0.1 to 1
- w_gate: bfloat16 [16, 4096, 2048], P('sp', None, 'tp'), may hold values from -0.09375 to 0.09375
- w_up: bfloat16 [16, 4096, 2048], P('sp', None, 'tp'), may hold values from -0.09375 to 0.09375
- w_down: bfloat16 [16, 2048, 4096], P('sp', 'tp'), may hold values from -0.125 to 0.125
- value_in: bfloat16 [4096, 2048], P('sp', 'tp'), may hold values from -6 to 6
- gate_in: bfloat16 [4096, 2048], P('sp', 'tp'), may hold values from -6 to 6
- conv_pre: bfloat16 [4096, 2048], P('sp', 'tp'), may hold values from -200 to 200
- ln_gain: float32 [2048], P('tp'), may hold values from 0.1 to 1.9
- conv_taps: float32 [31, 2048], P(None, 'tp'), may hold values from -1 to 1
- w_out: bfloat16 [2048, 4096], P('tp'), may hold values from -0.125 to 0.125
Outputs:
- grad_gate: float32 [16, 4096, 2048], P('sp', None, 'tp')
- grad_up: float32 [16, 4096, 2048], P('sp', None, 'tp')
- grad_down: float32 [16, 2048, 4096], P('sp', 'tp')
- grad_out: float32 [2048, 4096], P('tp', 'sp')
- value_grad: bfloat16 [4096, 2048], P('sp', 'tp')
- gate_grad: bfloat16 [4096, 2048], P('sp', 'tp')
Inputs may be any that keep to these rules, and one draw needn't show every extreme that they name: `routes`: each token names two different experts. Among the tokens of one index of sp no expert is named more than 48 times, and in every draw some expert exactly 48 times.
All inputs are finite; a program needn't handle non-finite values.
Results may differ from a plain program's by a relative error of at most 0.0071.
Values may be sent and summed in bfloat16 or wider, within the bound.
No kernel may reach another device: no remote copies, remote signals or barrier semaphores. Data moves between devices by JAX's collectives and lax.ppermute only.
A program may use at most 128 MiB of HBM per device.

v0:
```python
import jax
import jax.numpy as jnp
from jax import lax
from jax.sharding import PartitionSpec as P

EPSILON = 1e-06


def sent_to_all(value, axis):
    count = lax.axis_size(axis)
    return lax.all_to_all(
        jnp.broadcast_to(value[None], (count, *value.shape)), axis, 0, 0, tiled=True
    )


def of_everyone(value, axis):
    everything = sent_to_all(value, axis)
    return jnp.sum(everything, axis=0)


def in_one(arrays, axis):
    vector, at, gathered = (jnp.concatenate([a.reshape(-1) for a in arrays]), 0, [])
    total = of_everyone(vector, axis)
    for a in arrays:
        gathered.append(total[at : at + a.size].reshape(a.shape))
        at += a.size
    return tuple(gathered)


def side_by_side(arrays, axis, split_dim, concat_dim, along):
    both = jnp.concatenate(arrays, axis=along)
    out, at, gathered = (
        lax.all_to_all(both, axis, split_axis=split_dim, concat_axis=concat_dim, tiled=True),
        0,
        [],
    )
    for a in arrays:
        gathered.append(lax.slice_in_dim(out, at, at + a.shape[along], axis=along))
        at += a.shape[along]
    return tuple(gathered)


def in_one_piece(arrays, axis, dim, along):
    widths = [a.shape[along] for a in arrays]
    both = jnp.concatenate(arrays, axis=along)
    out = lax.all_gather(both, axis, axis=dim, tiled=True)
    return tuple(jnp.split(out, [sum(widths[:k]) for k in range(1, len(widths))], axis=along))


def cut_along(value, dim, count):
    shape = value.shape
    blocks = value.reshape(*shape[:dim], count, shape[dim] // count, *shape[dim + 1 :])
    return jnp.moveaxis(blocks, dim, 0)


def sent_and_summed(value, axis, dim):
    count = lax.axis_size(axis)
    blocks = lax.all_to_all(cut_along(value, dim, count), axis, 0, 0, tiled=True)
    return jnp.sum(blocks.astype(jnp.float32), axis=0)


def shifted(block, axis, distance):
    devices = range(lax.axis_size(axis))
    route = [(i - distance, i) for i in devices if i - distance in devices]
    return lax.ppermute(block, axis, route)


def silu_slope(values):
    logistic = jax.nn.sigmoid(values)
    return logistic * (1.0 + values * (1.0 - logistic))


def per_device(
    upstream,
    stream,
    norm_gain,
    routes,
    route_weights,
    w_gate,
    w_up,
    w_down,
    value_in,
    gate_in,
    conv_pre,
    ln_gain,
    conv_taps,
    w_out,
):
    tok_rows, width_part = stream.shape
    token_groups = lax.axis_size("sp")
    width_groups = lax.axis_size("tp")
    model_width = width_part * width_groups
    channels = conv_pre.shape[1] * width_groups
    tap_count = conv_taps.shape[0]
    capacity = 3 * tok_rows // token_groups
    experts = w_gate.shape[0] * token_groups
    slot_count = experts * capacity
    expert_rows = token_groups * capacity
    residual = stream.astype(jnp.float32)
    conv_vals = conv_pre.astype(jnp.float32)
    row_squares, conv_total, conv_squares = in_one(
        (
            jnp.sum(residual * residual, axis=1),
            jnp.sum(conv_vals, axis=1),
            jnp.sum(conv_vals * conv_vals, axis=1),
        ),
        "tp",
    )
    inverse = lax.rsqrt(row_squares / model_width + EPSILON)[:, None]
    normed = (norm_gain[None, :] * residual * inverse).astype(jnp.bfloat16)
    flat_experts = routes.reshape(-1)
    one_hot = (flat_experts[:, None] == jnp.arange(experts, dtype=jnp.int32)[None, :]).astype(
        jnp.int32
    )
    slot_rank = jnp.sum((jnp.cumsum(one_hot, axis=0) - one_hot) * one_hot, axis=1)
    slot_index = (flat_experts * capacity + slot_rank).reshape(tok_rows, 2)
    slot_ids = jnp.arange(slot_count, dtype=jnp.int32)[:, None]
    first_hit = slot_ids == slot_index[None, :, 0]
    second_hit = slot_ids == slot_index[None, :, 1]
    any_hit = jnp.logical_or(first_hit, second_hit)
    picker = any_hit.astype(jnp.bfloat16)
    slot_weight = jnp.sum(
        jnp.where(first_hit, route_weights[None, :, 0], 0.0)
        + jnp.where(second_hit, route_weights[None, :, 1], 0.0),
        axis=1,
    )
    token_iota = jnp.arange(tok_rows, dtype=jnp.int32)[None, :]
    slot_token = jnp.where(
        jnp.any(any_hit, axis=1), jnp.sum(jnp.where(any_hit, token_iota, 0), axis=1), tok_rows
    )
    columns = normed.shape[1]
    normed_pad = jnp.concatenate([normed, jnp.zeros((1, columns), jnp.bfloat16)], axis=0)
    upstream_pad = jnp.concatenate([upstream, jnp.zeros((1, columns), jnp.bfloat16)], axis=0)
    inputs = normed_pad[slot_token]
    cotangent = (upstream_pad[slot_token].astype(jnp.float32) * slot_weight[:, None]).astype(
        jnp.bfloat16
    )
    sent_inputs = inputs.reshape(experts, capacity, columns)
    sent_cotangent = cotangent.reshape(experts, capacity, columns)
    part_inputs, part_cotangent = side_by_side((sent_inputs, sent_cotangent), "sp", 0, 0, 1)
    inputs, cotangent = in_one_piece(
        (
            part_inputs.reshape(expert_rows, width_part),
            part_cotangent.reshape(expert_rows, width_part),
        ),
        "tp",
        1,
        0,
    )
    gate_mat = w_gate[0]
    upper_mat = w_up[0]
    down_mat = w_down[0]
    gate_pre = jnp.dot(inputs, gate_mat, preferred_element_type=jnp.float32)
    upper_pre = jnp.dot(inputs, upper_mat, preferred_element_type=jnp.float32)
    active = (jax.nn.silu(gate_pre) * upper_pre).astype(jnp.bfloat16)
    active_back = lax.dot_general(
        cotangent, down_mat, (((1,), (1,)), ((), ())), preferred_element_type=jnp.float32
    )
    gate_back = (active_back * upper_pre * silu_slope(gate_pre)).astype(jnp.bfloat16)
    upper_back = (active_back * jax.nn.silu(gate_pre)).astype(jnp.bfloat16)
    grad_gate = lax.dot_general(
        inputs, gate_back, (((0,), (0,)), ((), ())), preferred_element_type=jnp.float32
    )
    grad_up = lax.dot_general(
        inputs, upper_back, (((0,), (0,)), ((), ())), preferred_element_type=jnp.float32
    )
    grad_down = lax.dot_general(
        active, cotangent, (((0,), (0,)), ((), ())), preferred_element_type=jnp.float32
    )
    input_part = lax.dot_general(
        gate_back, gate_mat, (((1,), (1,)), ((), ())), preferred_element_type=jnp.float32
    ) + lax.dot_general(
        upper_back, upper_mat, (((1,), (1,)), ((), ())), preferred_element_type=jnp.float32
    )
    input_back = lax.psum_scatter(
        input_part.astype(jnp.bfloat16), "tp", scatter_dimension=1, tiled=True
    )
    returned = lax.all_to_all(
        input_back.reshape(token_groups, capacity, width_part),
        "sp",
        split_axis=0,
        concat_axis=0,
        tiled=True,
    )
    returned = returned.reshape(slot_count, width_part)
    token_back = lax.dot_general(
        picker, returned, (((0,), (0,)), ((), ())), preferred_element_type=jnp.float32
    )
    gained = norm_gain[None, :] * token_back
    inner_sum = of_everyone(jnp.sum(gained * residual, axis=1), "tp")
    norm_back = inverse * gained - residual * inverse**3 * (inner_sum / model_width)[:, None]
    stream_grad = (upstream.astype(jnp.float32) + norm_back).astype(jnp.bfloat16)
    full_grad = lax.all_gather(stream_grad, "tp", axis=1, tiled=True)
    mean_val = (conv_total / channels)[:, None]
    variance = (conv_squares / channels)[:, None] - mean_val * mean_val
    inv_std = lax.rsqrt(variance + EPSILON)
    centred = (conv_vals - mean_val) * inv_std
    scaled = centred * ln_gain[None, :]
    mixed_out = jax.nn.silu(scaled).astype(jnp.bfloat16)
    columns = full_grad
    grad_rows = sent_and_summed(
        lax.dot_general(
            columns, mixed_out, (((0,), (0,)), ((), ())), preferred_element_type=jnp.float32
        ).astype(jnp.bfloat16),
        "sp",
        0,
    )
    grad_out = grad_rows.T
    mixed_back = lax.dot_general(
        full_grad, w_out, (((1,), (1,)), ((), ())), preferred_element_type=jnp.float32
    )
    norm_in = mixed_back * silu_slope(scaled) * ln_gain[None, :]
    norm_total, norm_cross = in_one(
        (jnp.sum(norm_in, axis=1), jnp.sum(norm_in * centred, axis=1)), "tp"
    )
    conv_back = inv_std * (
        norm_in - (norm_total / channels)[:, None] - centred * (norm_cross / channels)[:, None]
    )
    next_rim = shifted(conv_back[: tap_count - 1], "sp", -1)
    padded = jnp.concatenate([conv_back, next_rim], axis=0)
    glu_back = jnp.zeros(conv_back.shape, jnp.float32)
    for tap_index in range(tap_count):
        offset = tap_count - 1 - tap_index
        glu_back = glu_back + conv_taps[tap_index][None, :] * padded[offset : offset + tok_rows]
    gate_sigma = jax.nn.sigmoid(gate_in.astype(jnp.float32))
    value_grad = (glu_back * gate_sigma).astype(jnp.bfloat16)
    gate_grad = (glu_back * value_in.astype(jnp.float32) * gate_sigma * (1.0 - gate_sigma)).astype(
        jnp.bfloat16
    )
    return (grad_gate[None], grad_up[None], grad_down[None], grad_out, value_grad, gate_grad)


def solution(mesh):
    return jax.shard_map(
        per_device,
        mesh=mesh,
        in_specs=(
            P("sp", "tp"),
            P("sp", "tp"),
            P("tp"),
            P("sp", None),
            P("sp", None),
            P("sp", None, "tp"),
            P("sp", None, "tp"),
            P("sp", "tp", None),
            P("sp", "tp"),
            P("sp", "tp"),
            P("sp", "tp"),
            P("tp"),
            P(None, "tp"),
            P("tp", None),
        ),
        out_specs=(
            P("sp", None, "tp"),
            P("sp", None, "tp"),
            P("sp", "tp", None),
            P("tp", "sp"),
            P("sp", "tp"),
            P("sp", "tp"),
        ),
        check_vma=False,
    )
```

profile of v0, /device:TPU:1, one launch (start us, length us, event | category | flops | bytes accessed | tf_op | source)
XLA Modules:
  0.0 325.8 jit_solution(10947476030596708137)
XLA Ops:
  7.2 1.1 copy.69
  8.3 1.0 convert_reduce_fusion.1
  10.0 10.0 %all-to-all-start = ((f32[16,1,768]{2,1,0:T(1,128)}), f32[16,1,768]{2,1,0:T(1,128)S(1)}, u32[]{:S(2)}, u32[]{:S(2)}) async-start(f32[16,1,768]{2,1,0:T(1,128)} %broadcast_in_dim.81), calls=%async_computation | async-start | bytes 98304 | tf_op jit(solution)/shard_map/all_to_all | solution.py:11
  21.1 1.2 reduce-window.6
  25.1 0.9 concatenate.23
  26.0 2.7 gather_fusion.1
  30.5 2.7 gather_fusion
  33.2 20.6 %all_to_all.33 = bf16[16,96,256]{2,1,0:T(8,128)(2,1)S(1)} all-to-all(bf16[16,96,256]{2,1,0:T(8,128)(2,1)S(1)} %pad_maximum_fusion), channel_id=1, replica_groups=mesh['sp'=16,'tp'=16] {'sp'}, dimensions={0} | all-to-all | bytes 1572864 | tf_op jit(solution)/shard_map/all_to_all | solution.py:33
  53.9 0.9 pad_maximum_fusion.1
  55.1 79.9 %all-gather.3.cloned.1.call-done = bf16[1536,4096]{1,0:T(8,128)(2,1)} async-done(((bf16[1536,256]{1,0:T(8,128)(2,1)}), bf16[1536,4096]{1,0:T(8,128)(2,1)}) %all-gather.3.cloned.1.call-update) | async-done | bytes 12582928 | tf_op jit(solution)/shard_map/all_gather | solution.py:46
  134.9 4.7 %fusion.9 = f32[768,128]{1,0:T(8,128)S(1)} fusion(bf16[1536,4096]{1,0:T(8,128)(2,1)} %all-gather.3.cloned.1.call-done, bf16[1,4096,128]{2,1,0:T(8,128)(2,1)S(1)} %copy-done), kind=kOutput, calls=%fused_computation.13 | convolution fusion | flops 805306368 | bytes 7733248 | tf_op jit(solution)/shard_map/dot_general | solution.py:153
  139.7 5.2 %fusion.11 = f32[768,128]{1,0:T(8,128)S(1)} fusion(bf16[1536,4096]{1,0:T(8,128)(2,1)} %all-gather.3.cloned.1.call-done, bf16[1,4096,128]{2,1,0:T(8,128)(2,1)S(1)} %copy-done.2), kind=kOutput, calls=%fused_computation.15 | convolution fusion | flops 805306368 | bytes 7733248 | tf_op jit(solution)/shard_map/dot_general | solution.py:154
  144.9 1.8 multiply_convert_fusion.1
  146.7 1.8 fusion.14
  148.5 4.4 %add_convert_fusion = bf16[768,4096]{1,0:T(8,128)(2,1)} fusion(f32[768,4096]{1,0:T(8,128)S(1)} %fusion.14, bf16[768,128]{1,0:T(8,128)(2,1)S(1)} %get-tuple-element.36, bf16[1,4096,128]{2,1,0:T(8,128)(2,1)S(1)} %copy-done.2), kind=kOutput, calls=%fused_computation.2 | convolution fusion | flops 811597824 | bytes 20119552 | tf_op jit(solution)/shard_map/dot_general | solution.py:172
  153.0 61.9 %reduce-scatter.2.cloned.1.call-done = bf16[768,256]{1,0:T(8,128)(2,1)} async-done(((bf16[768,4096]{1,0:T(8,128)(2,1)}), bf16[768,256]{1,0:T(8,128)(2,1)}) %reduce-scatter.2.cloned.1.call-update) | async-done | bytes 393232 | tf_op jit(solution)/shard_map/reduce_scatter | solution.py:175
  214.8 14.7 %all_to_all.34 = bf16[16,48,256]{2,1,0:T(8,128)(2,1)S(1)} all-to-all(bf16[16,48,256]{2,1,0:T(8,128)(2,1)} %bitcast.128), channel_id=1, replica_groups=mesh['sp'=16,'tp'=16] {'sp'}, dimensions={0} | all-to-all | bytes 786432 | tf_op jit(solution)/shard_map/all_to_all | solution.py:178
  230.6 9.6 %all-to-all-start.3 = ((f32[16,1,256]{2,1,0:T(1,128)}), f32[16,1,256]{2,1,0:T(1,128)S(1)}, u32[]{:S(2)}, u32[]{:S(2)}) async-start(f32[16,1,256]{2,1,0:T(1,128)} %broadcast_in_dim.93), calls=%async_computation.4 | async-start | bytes 32768 | tf_op jit(solution)/shard_map/all_to_all | solution.py:11
  240.6 7.0 %all-to-all-done.3 = f32[16,1,256]{2,1,0:T(1,128)S(1)} async-done(((f32[16,1,256]{2,1,0:T(1,128)}), f32[16,1,256]{2,1,0:T(1,128)S(1)}, u32[]{:S(2)}, u32[]{:S(2)}) %all-to-all-start.3) | async-done | bytes 16416 | tf_op jit(solution)/shard_map/all_to_all | solution.py:11
  249.6 5.9 %convolution_bitcast_fusion.1 = f32[1,4096,128]{2,1,0:T(8,128)} fusion(bf16[768,128]{1,0:T(8,128)(2,1)S(1)} %get-tuple-element.37, bf16[1536,4096]{1,0:T(8,128)(2,1)} %all-gather.3.cloned.1.call-done), kind=kOutput, calls=%fused_computation.9 | convolution fusion | flops 805306368 | bytes 8585216 | tf_op jit(solution)/shard_map/dot_general | solution.py:161
  255.5 6.1 %convolution_bitcast_fusion = f32[1,4096,128]{2,1,0:T(8,128)} fusion(bf16[768,128]{1,0:T(8,128)(2,1)S(1)} %get-tuple-element.36, bf16[1536,4096]{1,0:T(8,128)(2,1)} %all-gather.3.cloned.1.call-done), kind=kOutput, calls=%fused_computation.8 | convolution fusion | flops 805306368 | bytes 8585216 | tf_op jit(solution)/shard_map/dot_general | solution.py:164
  261.7 18.9 %all-gather.5.cloned.1.call-done = bf16[256,4096]{0,1:T(8,128)(2,1)} async-done(((bf16[256,256]{0,1:T(8,128)(2,1)}), bf16[256,4096]{0,1:T(8,128)(2,1)}) %all-gather.5.cloned.1.call-update) | async-done | bytes 2097168 | tf_op jit(solution)/shard_map/all_gather | solution.py:193
  280.6 2.5 fusion.154
  283.7 4.4 %all-to-all-start.5 = ((f32[16,1,512]{2,1,0:T(1,128)}), f32[16,1,512]{2,1,0:T(1,128)S(1)}, u32[]{:S(2)}, u32[]{:S(2)}) async-start(f32[16,1,512]{2,1,0:T(1,128)} %broadcast_in_dim.94), calls=%async_computation.6 | async-start | bytes 65536 | tf_op jit(solution)/shard_map/all_to_all | solution.py:11
  288.1 3.4 %convolution_convert_fusion = bf16[4096,128]{1,0:T(8,128)(2,1)} fusion(bf16[256,4096]{0,1:T(8,128)(2,1)} %all-gather.5.cloned.1.call-done, bf16[256,128]{1,0:T(8,128)(2,1)S(1)} %copy-done.3, f32[128]{0:T(128)S(1)} %copy-done.36, f32[256]{0:T(256)S(1)} %copy-done.9, f32[256]{0:T(256)S(1)} %copy-done.8), kind=kOutput, calls=%fused_computation.10 | convolution fusion | flops 269254656 | bytes 3213824 | tf_op jit(solution)/shard_map/dot_general | solution.py:202
  291.7 3.8 %all-to-all-done.5 = f32[16,1,512]{2,1,0:T(1,128)S(1)} async-done(((f32[16,1,512]{2,1,0:T(1,128)}), f32[16,1,512]{2,1,0:T(1,128)S(1)}, u32[]{:S(2)}, u32[]{:S(2)}) %all-to-all-start.5) | async-done | bytes 32800 | tf_op jit(solution)/shard_map/all_to_all | solution.py:11
  295.5 6.5 %all-to-all-start.4 = ((bf16[16,256,128]{2,1,0:T(8,128)(2,1)}), bf16[16,256,128]{2,1,0:T(8,128)(2,1)S(1)}, u32[]{:S(2)}, u32[]{:S(2)}) async-start(bf16[16,256,128]{2,1,0:T(8,128)(2,1)} %bitcast.17), calls=%async_computation.5 | async-start | bytes 2097152 | tf_op jit(solution)/shard_map/all_to_all | solution.py:58
  302.3 1.3 collective-permute-start
  303.6 5.2 %fusion.4 = f32[1,128,4096]{2,1,0:T(8,128)} fusion(bf16[1536,4096]{1,0:T(8,128)(2,1)} %all-gather.3.cloned.1.call-done, f32[768,128]{1,0:T(8,128)S(1)} %fusion.11, f32[768,128]{1,0:T(8,128)S(1)} %fusion.9), kind=kOutput, calls=%fused_computation.7 | convolution fusion | flops 805896192 | bytes 9175040 | tf_op jit(solution)/shard_map/dot_general | solution.py:167
  308.8 6.6 %collective-permute-done = f32[30,128]{1,0:T(8,128)S(1)} collective-permute-done((f32[30,128]{1,0:T(8,128)S(1)}, f32[30,128]{1,0:T(8,128)S(1)}, u32[]{:S(2)}, u32[]{:S(2)}) %collective-permute-start) | collective-permute-done | bytes 15392 | tf_op jit(solution)/shard_map/ppermute | solution.py:65
  315.6 1.1 multiply_convert_fusion.4
  317.5 0.9 all-to-all-done.4
  (133 shorter events, 12.7 us)
Async XLA Ops:
  7.2 127.7 %copy-start = (bf16[1,4096,128]{2,1,0:T(8,128)(2,1)S(1)}, bf16[1,4096,128]{2,1,0:T(8,128)(2,1)}, u32[]{:S(2)}) copy-start(bf16[1,4096,128]{2,1,0:T(8,128)(2,1)} %param.19) | copy-start | bytes 3145732
  10.0 18.9 %all-to-all-start = ((f32[16,1,768]{2,1,0:T(1,128)}), f32[16,1,768]{2,1,0:T(1,128)S(1)}, u32[]{:S(2)}, u32[]{:S(2)}) async-start(f32[16,1,768]{2,1,0:T(1,128)} %broadcast_in_dim.81), calls=%async_computation | async-start | bytes 98304 | tf_op jit(solution)/shard_map/all_to_all | solution.py:11
  20.0 115.0 %all-gather.3.cloned.1.call-start = ((), (), s32[]{:S(2)}) async-start(), calls=%async_computation.7 | async-start | bytes 13369344 | tf_op jit(solution)/shard_map/all_gather | solution.py:46
  53.9 85.8 %copy-start.2 = (bf16[1,4096,128]{2,1,0:T(8,128)(2,1)S(1)}, bf16[1,4096,128]{2,1,0:T(8,128)(2,1)}, u32[]{:S(2)}) copy-start(bf16[1,4096,128]{2,1,0:T(8,128)(2,1)} %param.20) | copy-start | bytes 3145732
  54.8 160.0 %reduce-scatter.2.cloned.1.call-start = ((), (), s32[]{:S(2)}) async-start(), calls=%async_computation.8 | async-start | bytes 6684672 | tf_op jit(solution)/shard_map/reduce_scatter | solution.py:175
  153.0 76.6 %copy-start.35 = (f32[256]{0:T(256)S(1)}, f32[256]{0:T(256)}, u32[]{:S(2)}) copy-start(f32[256]{0:T(256)} %param.16) | copy-start | bytes 3076
  153.0 87.5 %copy-start.4 = (bf16[256,256]{1,0:T(8,128)(2,1)S(1)}, bf16[256,256]{1,0:T(8,128)(2,1)}, u32[]{:S(2)}) copy-start(bf16[256,256]{1,0:T(8,128)(2,1)} %param.14) | copy-start | bytes 393220
  153.0 94.6 %copy-start.10 = (f32[256]{0:T(256)S(1)}, f32[256]{0:T(256)}, u32[]{:S(2)}) copy-start(f32[256]{0:T(256)} %get-tuple-element.72) | copy-start | bytes 3076
  153.0 95.4 %copy-start.7 = (f32[31,128]{1,0:T(8,128)S(1)}, f32[31,128]{1,0:T(8,128)}, u32[]{:S(2)}) copy-start(f32[31,128]{1,0:T(8,128)} %param.26) | copy-start | bytes 47620
  230.6 16.9 %all-to-all-start.3 = ((f32[16,1,256]{2,1,0:T(1,128)}), f32[16,1,256]{2,1,0:T(1,128)S(1)}, u32[]{:S(2)}, u32[]{:S(2)}) async-start(f32[16,1,256]{2,1,0:T(1,128)} %broadcast_in_dim.93), calls=%async_computation.4 | async-start | bytes 32768 | tf_op jit(solution)/shard_map/all_to_all | solution.py:11
  240.2 40.4 %all-gather.5.cloned.1.call-start = ((), (), s32[]{:S(2)}) async-start(), calls=%async_computation.9 | async-start | bytes 2228224 | tf_op jit(solution)/shard_map/all_gather | solution.py:193
  255.5 25.1 %copy-start.3 = (bf16[256,128]{1,0:T(8,128)(2,1)S(1)}, bf16[256,128]{1,0:T(8,128)(2,1)}, u32[]{:S(2)}) copy-start(bf16[256,128]{1,0:T(8,128)(2,1)} %param.24) | copy-start | bytes 196612
  255.5 25.1 %copy-start.8 = (f32[256]{0:T(256)S(1)}, f32[256]{0:T(256)}, u32[]{:S(2)}) copy-start(f32[256]{0:T(256)} %get-tuple-element.71) | copy-start | bytes 3076
  255.5 25.1 %copy-start.9 = (f32[256]{0:T(256)S(1)}, f32[256]{0:T(256)}, u32[]{:S(2)}) copy-start(f32[256]{0:T(256)} %get-tuple-element.74) | copy-start | bytes 3076
  255.5 25.1 %copy-start.36 = (f32[128]{0:T(128)S(1)}, f32[128]{0:T(128)}, u32[]{:S(2)}) copy-start(f32[128]{0:T(128)} %param.25) | copy-start | bytes 1540
  255.5 25.1 %copy-start.38 = (bf16[128,4096]{1,0:T(8,128)(2,1)S(1)}, bf16[128,4096]{1,0:T(8,128)(2,1)}, u32[]{:S(2)}) copy-start(bf16[128,4096]{1,0:T(8,128)(2,1)} %param.27) | copy-start | bytes 3145732
  283.7 11.8 %all-to-all-start.5 = ((f32[16,1,512]{2,1,0:T(1,128)}), f32[16,1,512]{2,1,0:T(1,128)S(1)}, u32[]{:S(2)}, u32[]{:S(2)}) async-start(f32[16,1,512]{2,1,0:T(1,128)} %broadcast_in_dim.94), calls=%async_computation.6 | async-start | bytes 65536 | tf_op jit(solution)/shard_map/all_to_all | solution.py:11
  291.5 23.9 %copy-start.13 = (f32[128]{0:T(128)S(1)}, f32[128]{0:T(128)}, u32[]{:S(2)}) copy-start(f32[128]{0:T(128)} %get-tuple-element.68) | copy-start | bytes 1540
  291.5 23.9 %copy-start.14 = (f32[128]{0:T(128)S(1)}, f32[128]{0:T(128)}, u32[]{:S(2)}) copy-start(f32[128]{0:T(128)} %get-tuple-element.69) | copy-start | bytes 1540
  291.5 23.9 %copy-start.15 = (f32[128]{0:T(128)S(1)}, f32[128]{0:T(128)}, u32[]{:S(2)}) copy-start(f32[128]{0:T(128)} %get-tuple-element.70) | copy-start | bytes 1540
  291.6 23.9 %copy-start.16 = (f32[128]{0:T(128)S(1)}, f32[128]{0:T(128)}, u32[]{:S(2)}) copy-start(f32[128]{0:T(128)} %get-tuple-element.40) | copy-start | bytes 1540
  291.6 23.9 %copy-start.17 = (f32[128]{0:T(128)S(1)}, f32[128]{0:T(128)}, u32[]{:S(2)}) copy-start(f32[128]{0:T(128)} %get-tuple-element.41) | copy-start | bytes 1540
  291.6 23.9 %copy-start.18 = (f32[128]{0:T(128)S(1)}, f32[128]{0:T(128)}, u32[]{:S(2)}) copy-start(f32[128]{0:T(128)} %get-tuple-element.42) | copy-start | bytes 1540
  291.6 23.9 %copy-start.19 = (f32[128]{0:T(128)S(1)}, f32[128]{0:T(128)}, u32[]{:S(2)}) copy-start(f32[128]{0:T(128)} %get-tuple-element.43) | copy-start | bytes 1540
  291.6 23.9 %copy-start.20 = (f32[128]{0:T(128)S(1)}, f32[128]{0:T(128)}, u32[]{:S(2)}) copy-start(f32[128]{0:T(128)} %get-tuple-element.44) | copy-start | bytes 1540
  291.6 23.9 %copy-start.21 = (f32[128]{0:T(128)S(1)}, f32[128]{0:T(128)}, u32[]{:S(2)}) copy-start(f32[128]{0:T(128)} %get-tuple-element.45) | copy-start | bytes 1540
  291.6 23.9 %copy-start.22 = (f32[128]{0:T(128)S(1)}, f32[128]{0:T(128)}, u32[]{:S(2)}) copy-start(f32[128]{0:T(128)} %get-tuple-element.46) | copy-start | bytes 1540
  291.6 23.9 %copy-start.23 = (f32[128]{0:T(128)S(1)}, f32[128]{0:T(128)}, u32[]{:S(2)}) copy-start(f32[128]{0:T(128)} %get-tuple-element.47) | copy-start | bytes 1540
  291.6 23.9 %copy-start.24 = (f32[128]{0:T(128)S(1)}, f32[128]{0:T(128)}, u32[]{:S(2)}) copy-start(f32[128]{0:T(128)} %get-tuple-element.48) | copy-start | bytes 1540
  291.6 23.9 %copy-start.25 = (f32[128]{0:T(128)S(1)}, f32[128]{0:T(128)}, u32[]{:S(2)}) copy-start(f32[128]{0:T(128)} %get-tuple-element.49) | copy-start | bytes 1540
  295.5 22.9 %all-to-all-start.4 = ((bf16[16,256,128]{2,1,0:T(8,128)(2,1)}), bf16[16,256,128]{2,1,0:T(8,128)(2,1)S(1)}, u32[]{:S(2)}, u32[]{:S(2)}) async-start(bf16[16,256,128]{2,1,0:T(8,128)(2,1)} %bitcast.17), calls=%async_computation.5 | async-start | bytes 2097152 | tf_op jit(solution)/shard_map/all_to_all | solution.py:58
  302.3 13.1 %collective-permute-start = (f32[30,128]{1,0:T(8,128)S(1)}, f32[30,128]{1,0:T(8,128)S(1)}, u32[]{:S(2)}, u32[]{:S(2)}) collective-permute-start(f32[30,128]{1,0:T(8,128)S(1)} %slice.309), channel_id=1, source_target_pairs={{16,0},{32,16},{48,32},{64,48},{80,64},{96,80},{112,96},{128,112},... | collective-permute-start | bytes 46088 | tf_op jit(solution)/shard_map/ppermute | solution.py:65
  (15 other events, 325.7 us)
Sparse Core Ops, SparseCore 0:
  55.0 79.9 all-gather.2
  153.1 61.6 reduce-scatter.1
  248.5 32.0 all-gather.4
where the time goes:
time: 327 us; the launch traced here: 326 us
  waiting for transfers between devices  179 us (55%)
  matrix products  41.5 us (13%)
  blocking collectives  35.4 us (11%)
  starting transfers between devices  32.3 us (10%)
  between operations  14.4 us (4%)
  local copies, waits for them, and re-layouts  14 us (4%)
  other arithmetic  9.31 us (3%)
    all_gather x1, waiting for transfers between devices, in_one_piece(): out = lax.all_gather(both, axis, axis=dim, tiled=True)  79.9 us
    reduce_scatter x1, waiting for transfers between devices, per_device(): lax.psum_scatter(input_part.astype(jnp.bfloat16), 'tp', scatter_dimension...  61.9 us
    all_to_all x3, starting transfers between devices, sent_to_all(): lax.all_to_all(jnp.broadcast_to(value[None], (count, *value.shape)), axis...  23.9 us
    all_to_all x1, blocking collectives, side_by_side(): lax.all_to_all(both, axis, split_axis=split_dim, concat_axis=concat_dim,...  20.6 us
    all_gather x1, waiting for transfers between devices, per_device(): full_grad = lax.all_gather(stream_grad, 'tp', axis=1, tiled=True)  18.9 us
    all_to_all x1, blocking collectives, per_device(): lax.all_to_all(input_back.reshape(token_groups, capacity, width_part), 's...  14.7 us
    all_to_all x3, waiting for transfers between devices, sent_to_all(): lax.all_to_all(jnp.broadcast_to(value[None], (count, *value.shape)), axis...  10.7 us
    ppermute x1, waiting for transfers between devices, shifted(): return lax.ppermute(block, axis, route)  6.6 us
  transfers between devices with their start and end apart: 8, of which 7 were waited for; matrix products, arithmetic and copies ran while one was open for 10% of the time, Pallas kernels for 0%

commit v1 on v0

--- a/solution.py
+++ b/solution.py
@@ -190,7 +190,9 @@
     inner_sum = of_everyone(jnp.sum(gained * residual, axis=1), "tp")
     norm_back = inverse * gained - residual * inverse**3 * (inner_sum / model_width)[:, None]
     stream_grad = (upstream.astype(jnp.float32) + norm_back).astype(jnp.bfloat16)
-    full_grad = lax.all_gather(stream_grad, "tp", axis=1, tiled=True)
+    full_grad = jnp.concatenate(
+        lax.all_to_all(jnp.stack([stream_grad] * lax.axis_size("tp")), "tp", 0, 0), axis=1
+    )
     mean_val = (conv_total / channels)[:, None]
     variance = (conv_squares / channels)[:, None] - mean_val * mean_val
     inv_std = lax.rsqrt(variance + EPSILON)

time: 327 us -> 346 us (1.058)
  waiting for transfers between devices: 179 us -> 200 us
    all_to_all x0 -> x1, waiting for transfers between devices: none -> 37.2 us  [per_device(): lax.all_to_all(jnp.stack([stream_grad] * lax.axis_size('tp')), 'tp', 0, 0)]
    all_gather x1 -> x0, waiting for transfers between devices: 18.9 us -> none  [per_device(): full_grad = lax.all_gather(stream_grad, 'tp', axis=1, tiled=True)]
    all_to_all x0 -> x1, starting transfers between devices: none -> 3.9 us  [per_device(): lax.all_to_all(jnp.stack([stream_grad] * lax.axis_size('tp')), 'tp', 0, 0)]
  transfers between devices with their start and end apart: 8 -> 8, of which waited for: 7 -> 7; matrix products, arithmetic and copies ran while one was open for 10% -> 9% of each run, Pallas kernels for 0% -> 0%
where the time goes in v1:
time: 346 us; the launch traced here: 345 us
  waiting for transfers between devices  200 us (58%)
  matrix products  39.8 us (12%)
  blocking collectives  35.2 us (10%)
  starting transfers between devices  33.5 us (10%)
  between operations  14.4 us (4%)
  local copies, waits for them, and re-layouts  14.2 us (4%)
  other arithmetic  8.03 us (2%)
    all_gather x1, waiting for transfers between devices, in_one_piece(): out = lax.all_gather(both, axis, axis=dim, tiled=True)  79.9 us
    reduce_scatter x1, waiting for transfers between devices, per_device(): lax.psum_scatter(input_part.astype(jnp.bfloat16), 'tp', scatter_dimension...  62 us
    all_to_all x1, waiting for transfers between devices, per_device(): lax.all_to_all(jnp.stack([stream_grad] * lax.axis_size('tp')), 'tp', 0, 0)  37.2 us
    all_to_all x3, starting transfers between devices, sent_to_all(): lax.all_to_all(jnp.broadcast_to(value[None], (count, *value.shape)), axis...  24.4 us
    all_to_all x1, blocking collectives, side_by_side(): lax.all_to_all(both, axis, split_axis=split_dim, concat_axis=concat_dim,...  20.6 us
    all_to_all x1, blocking collectives, per_device(): lax.all_to_all(input_back.reshape(token_groups, capacity, width_part), 's...  14.6 us
    all_to_all x3, waiting for transfers between devices, sent_to_all(): lax.all_to_all(jnp.broadcast_to(value[None], (count, *value.shape)), axis...  12.7 us
  transfers between devices with their start and end apart: 8, of which 7 were waited for; matrix products, arithmetic and copies ran while one was open for 9% of the time, Pallas kernels for 0%

profile of v1, /device:TPU:1, one launch (start us, length us, event | category | flops | bytes accessed | tf_op | source)
XLA Modules:
  0.0 345.0 jit_solution(11315314069520617895)
XLA Ops:
  7.2 1.1 copy.70
  8.3 1.0 convert_reduce_fusion.1
  10.0 10.0 %all-to-all-start = ((f32[16,1,768]{2,1,0:T(1,128)}), f32[16,1,768]{2,1,0:T(1,128)S(1)}, u32[]{:S(2)}, u32[]{:S(2)}) async-start(f32[16,1,768]{2,1,0:T(1,128)} %broadcast_in_dim.81), calls=%async_computation | async-start | bytes 98304 | tf_op jit(solution)/shard_map/all_to_all | solution.py:11
  21.1 1.2 reduce-window.6
  26.0 2.7 gather_fusion.1
  29.9 2.7 gather_fusion
  32.6 20.6 %all_to_all.38 = bf16[16,96,256]{2,1,0:T(8,128)(2,1)S(1)} all-to-all(bf16[16,96,256]{2,1,0:T(8,128)(2,1)S(1)} %pad_maximum_fusion), channel_id=1, replica_groups=mesh['sp'=16,'tp'=16] {'sp'}, dimensions={0} | all-to-all | bytes 1572864 | tf_op jit(solution)/shard_map/all_to_all | solution.py:33
  54.5 79.9 %all-gather.2.cloned.1.call-done = bf16[1536,4096]{1,0:T(8,128)(2,1)} async-done(((bf16[1536,256]{1,0:T(8,128)(2,1)}), bf16[1536,4096]{1,0:T(8,128)(2,1)}) %all-gather.2.cloned.1.call-update) | async-done | bytes 12582928 | tf_op jit(solution)/shard_map/all_gather | solution.py:46
  134.3 4.7 %fusion.9 = f32[768,128]{1,0:T(8,128)S(1)} fusion(bf16[1536,4096]{1,0:T(8,128)(2,1)} %all-gather.2.cloned.1.call-done, bf16[1,4096,128]{2,1,0:T(8,128)(2,1)S(1)} %copy-done), kind=kOutput, calls=%fused_computation.13 | convolution fusion | flops 805306368 | bytes 7733248 | tf_op jit(solution)/shard_map/dot_general | solution.py:153
  139.1 5.4 %fusion.11 = f32[768,128]{1,0:T(8,128)S(1)} fusion(bf16[1536,4096]{1,0:T(8,128)(2,1)} %all-gather.2.cloned.1.call-done, bf16[1,4096,128]{2,1,0:T(8,128)(2,1)S(1)} %copy-done.2), kind=kOutput, calls=%fused_computation.15 | convolution fusion | flops 805306368 | bytes 7733248 | tf_op jit(solution)/shard_map/dot_general | solution.py:154
  144.5 1.8 multiply_convert_fusion.1
  146.3 1.8 fusion.14
  148.1 4.5 %add_convert_fusion = bf16[768,4096]{1,0:T(8,128)(2,1)} fusion(f32[768,4096]{1,0:T(8,128)S(1)} %fusion.14, bf16[768,128]{1,0:T(8,128)(2,1)S(1)} %get-tuple-element.36, bf16[1,4096,128]{2,1,0:T(8,128)(2,1)S(1)} %copy-done.2), kind=kOutput, calls=%fused_computation.2 | convolution fusion | flops 811597824 | bytes 20119552 | tf_op jit(solution)/shard_map/dot_general | solution.py:172
  152.6 62.0 %reduce-scatter.2.cloned.1.call-done = bf16[768,256]{1,0:T(8,128)(2,1)} async-done(((bf16[768,4096]{1,0:T(8,128)(2,1)}), bf16[768,256]{1,0:T(8,128)(2,1)}) %reduce-scatter.2.cloned.1.call-update) | async-done | bytes 393232 | tf_op jit(solution)/shard_map/reduce_scatter | solution.py:175
  214.7 14.6 %all_to_all.39 = bf16[16,48,256]{2,1,0:T(8,128)(2,1)S(1)} all-to-all(bf16[16,48,256]{2,1,0:T(8,128)(2,1)} %bitcast.134), channel_id=1, replica_groups=mesh['sp'=16,'tp'=16] {'sp'}, dimensions={0} | all-to-all | bytes 786432 | tf_op jit(solution)/shard_map/all_to_all | solution.py:178
  230.3 9.6 %all-to-all-start.3 = ((f32[16,1,256]{2,1,0:T(1,128)}), f32[16,1,256]{2,1,0:T(1,128)S(1)}, u32[]{:S(2)}, u32[]{:S(2)}) async-start(f32[16,1,256]{2,1,0:T(1,128)} %broadcast_in_dim.93), calls=%async_computation.4 | async-start | bytes 32768 | tf_op jit(solution)/shard_map/all_to_all | solution.py:11
  240.0 7.2 %all-to-all-done.3 = f32[16,1,256]{2,1,0:T(1,128)S(1)} async-done(((f32[16,1,256]{2,1,0:T(1,128)}), f32[16,1,256]{2,1,0:T(1,128)S(1)}, u32[]{:S(2)}, u32[]{:S(2)}) %all-to-all-start.3) | async-done | bytes 16416 | tf_op jit(solution)/shard_map/all_to_all | solution.py:11
  247.3 1.5 stack.2
  248.9 3.9 %all-to-all-start.4 = ((bf16[16,256,256]{1,2,0:T(8,128)(2,1)}), bf16[16,256,256]{1,2,0:T(8,128)(2,1)S(1)}, u32[]{:S(2)}, u32[]{:S(2)}) async-start(bf16[16,256,256]{1,2,0:T(8,128)(2,1)} %stack.2), calls=%async_computation.5 | async-start | bytes 4194304 | tf_op jit(solution)/shard_map/all_to_all | solution.py:194
  252.8 5.9 %convolution_bitcast_fusion.1 = f32[1,4096,128]{2,1,0:T(8,128)} fusion(bf16[768,128]{1,0:T(8,128)(2,1)} %copy-done.8, bf16[1536,4096]{1,0:T(8,128)(2,1)} %all-gather.2.cloned.1.call-done), kind=kOutput, calls=%fused_computation.9 | convolution fusion | flops 805306368 | bytes 8585216 | tf_op jit(solution)/shard_map/dot_general | solution.py:161
  258.8 6.0 %convolution_bitcast_fusion = f32[1,4096,128]{2,1,0:T(8,128)} fusion(bf16[768,128]{1,0:T(8,128)(2,1)S(1)} %get-tuple-element.36, bf16[1536,4096]{1,0:T(8,128)(2,1)} %all-gather.2.cloned.1.call-done), kind=kOutput, calls=%fused_computation.8 | convolution fusion | flops 805306368 | bytes 8585216 | tf_op jit(solution)/shard_map/dot_general | solution.py:164
  264.7 37.2 %all-to-all-done.4 = bf16[16,256,256]{1,2,0:T(8,128)(2,1)S(1)} async-done(((bf16[16,256,256]{1,2,0:T(8,128)(2,1)}), bf16[16,256,256]{1,2,0:T(8,128)(2,1)S(1)}, u32[]{:S(2)}, u32[]{:S(2)}) %all-to-all-start.4) | async-done | bytes 2097184 | tf_op jit(solution)/shard_map/all_to_all | solution.py:194
  301.9 2.1 fusion.154
  304.6 4.8 %all-to-all-start.6 = ((f32[16,1,512]{2,1,0:T(1,128)}), f32[16,1,512]{2,1,0:T(1,128)S(1)}, u32[]{:S(2)}, u32[]{:S(2)}) async-start(f32[16,1,512]{2,1,0:T(1,128)} %broadcast_in_dim.94), calls=%async_computation.7 | async-start | bytes 65536 | tf_op jit(solution)/shard_map/all_to_all | solution.py:11
  309.5 1.9 convolution_convert_fusion
  311.3 5.5 %all-to-all-done.6 = f32[16,1,512]{2,1,0:T(1,128)S(1)} async-done(((f32[16,1,512]{2,1,0:T(1,128)}), f32[16,1,512]{2,1,0:T(1,128)S(1)}, u32[]{:S(2)}, u32[]{:S(2)}) %all-to-all-start.6) | async-done | bytes 32800 | tf_op jit(solution)/shard_map/all_to_all | solution.py:11
  316.8 3.7 %all-to-all-start.5 = ((bf16[16,256,128]{2,1,0:T(8,128)(2,1)}), bf16[16,256,128]{2,1,0:T(8,128)(2,1)S(1)}, u32[]{:S(2)}, u32[]{:S(2)}) async-start(bf16[16,256,128]{2,1,0:T(8,128)(2,1)} %bitcast.128), calls=%async_computation.6 | async-start | bytes 2097152 | tf_op jit(solution)/shard_map/all_to_all | solution.py:58
  320.8 1.3 collective-permute-start
  322.1 5.4 %fusion.4 = f32[1,128,4096]{2,1,0:T(8,128)} fusion(bf16[1536,4096]{1,0:T(8,128)(2,1)} %all-gather.2.cloned.1.call-done, f32[768,128]{1,0:T(8,128)} %copy-done.6, f32[768,128]{1,0:T(8,128)} %copy-done.5), kind=kOutput, calls=%fused_computation.7 | convolution fusion | flops 805896192 | bytes 9175040 | tf_op jit(solution)/shard_map/dot_general | solution.py:167
  327.5 6.5 %collective-permute-done = f32[30,128]{1,0:T(8,128)S(1)} collective-permute-done((f32[30,128]{1,0:T(8,128)S(1)}, f32[30,128]{1,0:T(8,128)S(1)}, u32[]{:S(2)}, u32[]{:S(2)}) %collective-permute-start) | collective-permute-done | bytes 15392 | tf_op jit(solution)/shard_map/ppermute | solution.py:65
  334.0 1.1 multiply_convert_fusion.4
  335.8 1.5 all-to-all-done.5
  (83 shorter events, 11.8 us)
Async XLA Ops:
  7.2 127.2 %copy-start = (bf16[1,4096,128]{2,1,0:T(8,128)(2,1)S(1)}, bf16[1,4096,128]{2,1,0:T(8,128)(2,1)}, u32[]{:S(2)}) copy-start(bf16[1,4096,128]{2,1,0:T(8,128)(2,1)} %param.19) | copy-start | bytes 3145732
  10.0 18.9 %all-to-all-start = ((f32[16,1,768]{2,1,0:T(1,128)}), f32[16,1,768]{2,1,0:T(1,128)S(1)}, u32[]{:S(2)}, u32[]{:S(2)}) async-start(f32[16,1,768]{2,1,0:T(1,128)} %broadcast_in_dim.81), calls=%async_computation | async-start | bytes 98304 | tf_op jit(solution)/shard_map/all_to_all | solution.py:11
  20.0 114.4 %all-gather.2.cloned.1.call-start = ((), (), s32[]{:S(2)}) async-start(), calls=%async_computation.8 | async-start | bytes 13369344 | tf_op jit(solution)/shard_map/all_gather | solution.py:46
  53.3 85.8 %copy-start.2 = (bf16[1,4096,128]{2,1,0:T(8,128)(2,1)S(1)}, bf16[1,4096,128]{2,1,0:T(8,128)(2,1)}, u32[]{:S(2)}) copy-start(bf16[1,4096,128]{2,1,0:T(8,128)(2,1)} %param.20) | copy-start | bytes 3145732
  54.3 160.4 %reduce-scatter.2.cloned.1.call-start = ((), (), s32[]{:S(2)}) async-start(), calls=%async_computation.9 | async-start | bytes 6684672 | tf_op jit(solution)/shard_map/reduce_scatter | solution.py:175
  134.3 10.1 %copy-start.1 = (bf16[1536,4096]{1,0:T(8,128)(2,1)S(1)}, bf16[1536,4096]{1,0:T(8,128)(2,1)}, u32[]{:S(2)}) copy-start(bf16[1536,4096]{1,0:T(8,128)(2,1)} %all-gather.2.cloned.1.call-done) | copy-start | bytes 37748740
  139.1 9.1 %copy-start.5 = (f32[768,128]{1,0:T(8,128)}, f32[768,128]{1,0:T(8,128)S(1)}, u32[]{:S(2)}) copy-start(f32[768,128]{1,0:T(8,128)S(1)} %fusion.9) | copy-start | bytes 1179652
  139.1 5.4 %copy-start.13 = (bf16[1,128,4096]{2,1,0:T(8,128)(2,1)S(1)}, bf16[1,128,4096]{2,1,0:T(8,128)(2,1)}, u32[]{:S(2)}) copy-start(bf16[1,128,4096]{2,1,0:T(8,128)(2,1)} %param.21) | copy-start | bytes 3145732
  144.5 1.8 copy-start.6
  146.3 1.8 copy-start.8
  152.6 76.7 %copy-start.11 = (f32[256]{0:T(256)S(1)}, f32[256]{0:T(256)}, u32[]{:S(2)}) copy-start(f32[256]{0:T(256)} %param.16) | copy-start | bytes 3076
  152.6 87.3 %copy-start.4 = (bf16[256,256]{1,0:T(8,128)(2,1)S(1)}, bf16[256,256]{1,0:T(8,128)(2,1)}, u32[]{:S(2)}) copy-start(bf16[256,256]{1,0:T(8,128)(2,1)} %param.14) | copy-start | bytes 393220
  152.6 100.1 %copy-start.10 = (f32[31,128]{1,0:T(8,128)S(1)}, f32[31,128]{1,0:T(8,128)}, u32[]{:S(2)}) copy-start(f32[31,128]{1,0:T(8,128)} %param.26) | copy-start | bytes 47620
  230.3 16.9 %all-to-all-start.3 = ((f32[16,1,256]{2,1,0:T(1,128)}), f32[16,1,256]{2,1,0:T(1,128)S(1)}, u32[]{:S(2)}, u32[]{:S(2)}) async-start(f32[16,1,256]{2,1,0:T(1,128)} %broadcast_in_dim.93), calls=%async_computation.4 | async-start | bytes 32768 | tf_op jit(solution)/shard_map/all_to_all | solution.py:11
  248.9 53.0 %all-to-all-start.4 = ((bf16[16,256,256]{1,2,0:T(8,128)(2,1)}), bf16[16,256,256]{1,2,0:T(8,128)(2,1)S(1)}, u32[]{:S(2)}, u32[]{:S(2)}) async-start(bf16[16,256,256]{1,2,0:T(8,128)(2,1)} %stack.2), calls=%async_computation.5 | async-start | bytes 4194304 | tf_op jit(solution)/shard_map/all_to_all | solution.py:194
  258.8 43.1 %copy-start.3 = (bf16[256,128]{1,0:T(8,128)(2,1)S(1)}, bf16[256,128]{1,0:T(8,128)(2,1)}, u32[]{:S(2)}) copy-start(bf16[256,128]{1,0:T(8,128)(2,1)} %param.24) | copy-start | bytes 196612
  258.8 43.1 %copy-start.12 = (f32[128]{0:T(128)S(1)}, f32[128]{0:T(128)}, u32[]{:S(2)}) copy-start(f32[128]{0:T(128)} %param.25) | copy-start | bytes 1540
  304.6 12.2 %all-to-all-start.6 = ((f32[16,1,512]{2,1,0:T(1,128)}), f32[16,1,512]{2,1,0:T(1,128)S(1)}, u32[]{:S(2)}, u32[]{:S(2)}) async-start(f32[16,1,512]{2,1,0:T(1,128)} %broadcast_in_dim.94), calls=%async_computation.7 | async-start | bytes 65536 | tf_op jit(solution)/shard_map/all_to_all | solution.py:11
  311.3 22.7 %copy-start.7 = (bf16[256,128]{1,0:T(8,128)(2,1)S(1)}, bf16[256,128]{1,0:T(8,128)(2,1)}, u32[]{:S(2)}) copy-start(bf16[256,128]{1,0:T(8,128)(2,1)} %param.23) | copy-start | bytes 196612
  311.3 22.7 %copy-start.9 = (bf16[256,128]{1,0:T(8,128)(2,1)S(1)}, bf16[256,128]{1,0:T(8,128)(2,1)}, u32[]{:S(2)}) copy-start(bf16[256,128]{1,0:T(8,128)(2,1)} %param.22) | copy-start | bytes 196612
  316.8 20.5 %all-to-all-start.5 = ((bf16[16,256,128]{2,1,0:T(8,128)(2,1)}), bf16[16,256,128]{2,1,0:T(8,128)(2,1)S(1)}, u32[]{:S(2)}, u32[]{:S(2)}) async-start(bf16[16,256,128]{2,1,0:T(8,128)(2,1)} %bitcast.128), calls=%async_computation.6 | async-start | bytes 2097152 | tf_op jit(solution)/shard_map/all_to_all | solution.py:58
  320.8 13.2 %collective-permute-start = (f32[30,128]{1,0:T(8,128)S(1)}, f32[30,128]{1,0:T(8,128)S(1)}, u32[]{:S(2)}, u32[]{:S(2)}) collective-permute-start(f32[30,128]{1,0:T(8,128)S(1)} %slice.309), channel_id=1, source_target_pairs={{16,0},{32,16},{48,32},{64,48},{80,64},{96,80},{112,96},{128,112},... | collective-permute-start | bytes 46088 | tf_op jit(solution)/shard_map/ppermute | solution.py:65
Sparse Core Ops, SparseCore 0:
  54.4 79.9 all-gather.1
  152.8 61.8 reduce-scatter.1
